TPU v7x, 32 devices: a whole 2x2x4 slice. The times are simulated.
32 devices in a mesh: ep: 32 (over z, y, x, core).
Axes of the slice: x: 2, y: 2, z: 4, core: 2. Of those that a mesh axis runs over, the one named last changes fastest.
Arguments:
- tokens: bfloat16 [1024, 2048], P('ep'), may hold values from -6 to 6
- gain_mix: float32 [2048], replicated, may hold values from 0.1 to 1.9
- w_query: bfloat16 [2048, 384], replicated, may hold values from -0.125 to 0.125
- w_key: bfloat16 [2048, 384], replicated, may hold values from -0.125 to 0.125
- w_value: bfloat16 [2048, 768], replicated, may hold values from -0.125 to 0.125
- w_input_gate: bfloat16 [2048, 4], replicated, may hold values from -0.125 to 0.125
- w_forget_gate: bfloat16 [2048, 4], replicated, may hold values from -0.125 to 0.125
- bias_input: float32 [4], replicated, may hold values from -1 to 1
- bias_forget: float32 [4], replicated, may hold values from 0 to 5
- memory_cells: float32 [1024, 4, 96, 192], P('ep'), may hold values from -6 to 6
- normalizer: float32 [1024, 4, 96], P('ep'), may hold values from -6 to 6
- stabilizer: float32 [1024, 4], P('ep'), may hold values from -1 to 1
- w_mix_out: bfloat16 [768, 2048], replicated, may hold values from -0.21875 to 0.21875
- gain_mix_post: float32 [2048], replicated, may hold values from 0.1 to 1.9
- gain_ffn: float32 [2048], replicated, may hold values from 0.1 to 1.9
- w_router: bfloat16 [2048, 8], replicated, may hold values from -0.125 to 0.125
- routing: int32 [1024, 2], replicated, may hold values from 0 to 7, all different within a row; in each aligned block of 32 rows (0 to 31, 32 to 63, ...) at most 16 rows name the same one
- w_expert_gate: bfloat16 [32, 2048, 384], P('ep'), may hold values from -0.125 to 0.125
- w_expert_up: bfloat16 [32, 2048, 384], P('ep'), may hold values from -0.125 to 0.125
- w_expert_down: bfloat16 [32, 384, 2048], P('ep'), may hold values from -0.15625 to 0.15625
- gain_ffn_post: float32 [2048], replicated, may hold values from 0.1 to 1.9
Outputs:
- mixed: bfloat16 [1024, 2048], P('ep')
- cells_next: float32 [1024, 4, 96, 192], P('ep')
- normalizer_next: float32 [1024, 4, 96], P('ep')
- stabilizer_next: float32 [1024, 4], P('ep')
Inputs may be any that keep to these rules, and one draw needn't show every extreme that they name: `routing`: each row names 2 different experts. In the rows of one device (aligned blocks of 32 rows) no expert is named more than 16 times, a bound that some block reaches.
All inputs are finite; a program needn't handle non-finite values.
Results may differ from a plain program's by a relative error of at most 0.012.
Values may be sent and summed in bfloat16 or wider, within the bound.
A program may use at most 128 MiB of HBM per device.

v0:
```python
import jax
import jax.numpy as jnp
from jax import lax
from jax.sharding import PartitionSpec as P

epsilon = 1e-06


def normalize(values, gain):
    return values * lax.rsqrt(jnp.mean(values * values, axis=-1, keepdims=True) + epsilon) * gain


def rounded(values):
    return lax.optimization_barrier(values.astype(jnp.bfloat16)).astype(jnp.float32)


def cell_step(
    normed,
    w_query,
    w_key,
    w_value,
    w_input_gate,
    w_forget_gate,
    bias_input,
    bias_forget,
    memory_cells,
    normalizer,
    stabilizer,
):
    row_count, heads, key_size, value_size = memory_cells.shape
    query_rows = rounded(jnp.dot(normed, w_query, preferred_element_type=jnp.float32))
    query_rows = query_rows.reshape(row_count, heads, key_size) * key_size ** (-0.5)
    key_rows = rounded(jnp.dot(normed, w_key, preferred_element_type=jnp.float32)).reshape(
        row_count, heads, key_size
    )
    value_rows = rounded(jnp.dot(normed, w_value, preferred_element_type=jnp.float32)).reshape(
        row_count, heads, value_size
    )
    input_gate = jnp.dot(normed, w_input_gate, preferred_element_type=jnp.float32) + bias_input
    log_forget = jax.nn.log_sigmoid(
        jnp.dot(normed, w_forget_gate, preferred_element_type=jnp.float32) + bias_forget
    )
    carried = log_forget + stabilizer
    stab_next = jnp.maximum(carried, input_gate)
    keep_weight = jnp.exp(carried - stab_next)
    write_weight = jnp.exp(input_gate - stab_next)
    scaled_keys = write_weight[:, :, None] * key_rows
    cells_next = (
        keep_weight[:, :, None, None] * memory_cells
        + scaled_keys[:, :, :, None] * value_rows[:, :, None, :]
    )
    norm_next = keep_weight[:, :, None] * normalizer + scaled_keys
    numerator = jnp.einsum("bhd,bhde->bhe", query_rows, cells_next, precision=lax.Precision.HIGHEST)
    denominator = jnp.einsum("bhd,bhd->bh", query_rows, norm_next, precision=lax.Precision.HIGHEST)
    denominator = jnp.maximum(jnp.abs(denominator), jnp.exp(-stab_next))
    cell_out = (
        (numerator / denominator[:, :, None])
        .reshape(row_count, heads * value_size)
        .astype(jnp.bfloat16)
    )
    return (cell_out, cells_next, norm_next, stab_next)


def route_weights(rows_in, w_router, routes):
    logits = jnp.dot(rows_in, w_router, preferred_element_type=jnp.float32)
    onehot = routes[:, :, None] == jnp.arange(w_router.shape[1], dtype=jnp.int32)[None, None, :]
    chosen = jnp.sum(jnp.where(onehot, logits[:, None, :], 0.0), axis=-1)
    return jax.nn.sigmoid(chosen - chosen[:, ::-1])


def expert_quarter(row_block, gate_w, up_w, down_w):
    gate_part = jnp.dot(row_block, gate_w, preferred_element_type=jnp.float32)
    up_part = jnp.dot(row_block, up_w, preferred_element_type=jnp.float32)
    hidden = (jax.nn.silu(gate_part) * up_part).astype(jnp.bfloat16)
    return jnp.dot(hidden, down_w, preferred_element_type=jnp.float32).astype(jnp.bfloat16)


def body(
    tokens,
    gain_mix,
    w_query,
    w_key,
    w_value,
    w_input_gate,
    w_forget_gate,
    bias_input,
    bias_forget,
    memory_cells,
    normalizer,
    stabilizer,
    w_mix_out,
    gain_mix_post,
    gain_ffn,
    w_router,
    routing,
    w_expert_gate,
    w_expert_up,
    w_expert_down,
    gain_ffn_post,
):
    devices = lax.axis_size("ep")
    device_index = lax.axis_index("ep")
    seq_rows = tokens.shape[0]
    model_width = tokens.shape[1]
    experts = w_router.shape[1]
    group_size = devices // experts
    top_count = routing.shape[1]
    capacity = max(2, seq_rows * top_count * 2 // experts)
    residual = tokens.astype(jnp.float32)
    normed = normalize(residual, gain_mix).astype(jnp.bfloat16)
    cell_out, cells_next, norm_next, stab_next = cell_step(
        normed,
        w_query,
        w_key,
        w_value,
        w_input_gate,
        w_forget_gate,
        bias_input,
        bias_forget,
        memory_cells,
        normalizer,
        stabilizer,
    )
    mix_out = jnp.dot(cell_out, w_mix_out, preferred_element_type=jnp.float32)
    after_mix = (residual + normalize(mix_out, gain_mix_post)).astype(jnp.bfloat16)
    after_float = after_mix.astype(jnp.float32)
    expert_in = normalize(after_float, gain_ffn).astype(jnp.bfloat16)
    gate_w = w_expert_gate[0]
    up_w = w_expert_up[0]
    down_w = w_expert_down[0]
    own_routes = lax.dynamic_slice_in_dim(routing, device_index * seq_rows, seq_rows, 0)
    route_weight = route_weights(expert_in, w_router, own_routes)
    flat_routes = own_routes.reshape(-1)
    flat_hot = (flat_routes[:, None] == jnp.arange(experts, dtype=jnp.int32)[None, :]).astype(
        jnp.int32
    )
    slot_index = jnp.sum((jnp.cumsum(flat_hot, axis=0) - 1) * flat_hot, axis=1)
    position = flat_routes * capacity + slot_index
    dispatch = position[:, None] == jnp.arange(experts * capacity, dtype=jnp.int32)[None, :]
    repeated = jnp.repeat(expert_in, top_count, axis=0)
    outgoing = jnp.einsum(
        "rp,rd->pd", dispatch.astype(jnp.bfloat16), repeated, preferred_element_type=jnp.float32
    ).astype(jnp.bfloat16)
    outgoing = jnp.broadcast_to(
        outgoing.reshape(experts, 1, capacity, model_width),
        (experts, group_size, capacity, model_width),
    ).reshape(devices, capacity, model_width)
    arrived = lax.all_to_all(outgoing, "ep", split_axis=0, concat_axis=0, tiled=True)
    shape_in = arrived.shape
    computed = expert_quarter(arrived.reshape(-1, model_width), gate_w, up_w, down_w).reshape(
        shape_in
    )
    returned = lax.all_to_all(computed, "ep", split_axis=0, concat_axis=0, tiled=True)
    summed = jnp.sum(
        returned.astype(jnp.float32).reshape(experts, group_size, capacity, model_width), axis=1
    )
    summed = summed.reshape(experts * capacity, model_width)
    combine = jnp.where(dispatch, route_weight.reshape(-1)[:, None], 0.0)
    expert_rows = jnp.dot(combine, summed, precision=lax.Precision.HIGHEST)
    expert_sum = jnp.sum(expert_rows.reshape(seq_rows, top_count, model_width), axis=1)
    mixed = (after_float + normalize(expert_sum, gain_ffn_post)).astype(jnp.bfloat16)
    return (mixed, cells_next, norm_next, stab_next)


def solution(mesh):
    return jax.shard_map(
        body,
        mesh=mesh,
        in_specs=(
            P("ep", None),
            P(),
            P(),
            P(),
            P(),
            P(),
            P(),
            P(),
            P(),
            P("ep", None, None, None),
            P("ep", None, None),
            P("ep", None),
            P(),
            P(),
            P(),
            P(),
            P(),
            P("ep", None, None),
            P("ep", None, None),
            P("ep", None, None),
            P(),
        ),
        out_specs=(P("ep", None), P("ep", None, None, None), P("ep", None, None), P("ep", None)),
        check_vma=False,
    )
```

profile of v0, /device:TPU:0, one launch (start us, length us, event | category | flops | bytes accessed | tf_op | source)
XLA Modules:
  0.0 156.7 jit_solution(3638687667226925182)
XLA Ops:
  0.6 0.0 copy-start
  0.7 1.2 fusion.20
  1.9 1.9 %convolution_convert_fusion.4 = bf16[32,384]{1,0:T(8,128)(2,1)S(1)} fusion(bf16[2048,384]{1,0:T(8,128)(2,1)} %param.23, bf16[32,2048]{1,0:T(8,128)(2,1)} %param.21, f32[2048]{0:T(1024)} %param.22, f32[32]{0:T(128)S(1)} %add_rsqrt_fusion.3), kind=kOutput, calls=%fused_computation.14 | convolution fusion | flops 50606080 | bytes 1736832 | tf_op jit(solution)/shard_map/dot_general | solution.py:31
  3.8 0.1 reshape.149
  4.0 0.1 mul.166
  4.1 0.2 convolution_add_fusion
  4.3 0.2 subtract_exponential_fusion.1
  4.6 0.6 copy-done.15
  5.2 0.1 copy.39
  5.3 0.1 copy.40
  5.3 0.7 constant_dynamic-slice_fusion
  6.1 0.1 copy.52
  6.2 0.1 eq.61
  6.3 1.8 %convolution_convert_fusion.3 = bf16[32,384]{1,0:T(8,128)(2,1)S(1)} fusion(bf16[2048,384]{1,0:T(8,128)(2,1)} %param.24, bf16[32,2048]{1,0:T(8,128)(2,1)S(1)} %copy-done.2, f32[2048]{0:T(1024)S(1)} %copy-done.6, f32[32]{0:T(128)S(1)} %add_rsqrt_fusion.3), kind=kOutput, calls=%fused_computation.13 | convolution fusion | flops 50606080 | bytes 1736832 | tf_op jit(solution)/shard_map/dot_general | solution.py:33
  8.1 0.1 fusion.31
  8.2 0.1 reduce_window_sum.11
  8.3 0.8 select_reduce_fusion
  9.2 1.2 multiply_add_fusion.3
  10.4 0.7 reshape.145
  11.1 3.2 %convolution_convert_fusion.2 = bf16[32,768]{1,0:T(8,128)(2,1)} fusion(bf16[2048,768]{1,0:T(8,128)(2,1)} %param.25, bf16[32,2048]{1,0:T(8,128)(2,1)S(1)} %copy-done.2, f32[2048]{0:T(1024)S(1)} %copy-done.6, f32[32]{0:T(128)} %copy-done.17), kind=kOutput, calls=%fused_computation.12 | convolution fusion | flops 100950016 | bytes 3334272 | tf_op jit(solution)/shard_map/dot_general | solution.py:36
  14.4 0.8 multiply_reduce_fusion.2
  15.2 0.1 copy.51
  15.3 0.7 copy.42
  15.9 0.9 reshape.146
  16.9 6.1 %multiply_add_fusion = f32[32,4,96,192]{3,2,1,0:T(8,128)S(1)} fusion(f32[32,4,96,192]{3,2,1,0:T(8,128)} %param.30, f32[32,4,192]{2,1,0:T(4,128)S(1)} %reshape.146, f32[32,4,96]{2,1,0:T(4,128)S(1)} %get-tuple-element.8, f32[32,4]{1,0:T(8,128)} %copy-done.5), kind=kLoop, calls=%fused_computation | loop fusion | flops 7077888 | bytes 19022336 | tf_op jit(solution)/shard_map/add | solution.py:49
  23.0 6.1 %fusion.46 = f32[32,4,1,192]{3,2,1,0:T(1,128)S(1)} fusion(f32[32,4,96,1]{2,3,1,0:T(1,128)S(1)} %bitcast.54, f32[32,4,96,192]{3,2,1,0:T(8,128)S(1)} %multiply_add_fusion), kind=kOutput, calls=%fused_computation.75 | convolution fusion | flops 28311552 | bytes 9584640 | tf_op jit(solution)/shard_map/bhd,bhde->bhe/dot_general | solution.py:53
  29.1 0.1 fusion.28
  29.3 0.1 convert_element_type.59
  29.4 0.7 multiply_reduce_fusion.1
  30.2 0.2 fusion.24
  30.4 0.1 fusion.26
  30.5 0.9 broadcast_in_dim.30
  31.4 1.7 %reshape.137 = bf16[64,2048]{1,0:T(8,128)(2,1)} reshape(bf16[32,2,2048]{2,1,0:T(2,128)(2,1)} %broadcast_in_dim.30) | data formatting | bytes 524288 | tf_op jit(solution)/shard_map/reshape | solution.py:140
  33.1 1.4 convolution_convert_fusion.1
  34.5 0.2 broadcast_in_dim.32
  34.8 55.8 %all_to_all.10 = bf16[32,16,2048]{2,1,0:T(8,128)(2,1)S(1)} all-to-all(bf16[32,16,2048]{2,1,0:T(8,128)(2,1)S(1)} %bitcast.48), channel_id=1, replica_groups=mesh['ep'=32] {'ep'}, dimensions={0} | all-to-all | bytes 4194304 | tf_op jit(solution)/shard_map/all_to_all | solution.py:148
  90.6 1.3 copy-done.3
  91.9 2.1 %fusion.3 = f32[512,384]{1,0:T(8,128)} fusion(bf16[512,2048]{1,0:T(8,128)(2,1)S(1)} %bitcast.52, bf16[1,2048,384]{2,1,0:T(8,128)(2,1)S(1)} %copy-done.22), kind=kOutput, calls=%fused_computation.7 | convolution fusion | flops 805306368 | bytes 4456448 | tf_op jit(solution)/shard_map/dot_general | solution.py:72
  94.0 6.4 %convolution_convert_fusion = bf16[512,2048]{1,0:T(8,128)(2,1)} fusion(bf16[1,384,2048]{2,1,0:T(8,128)(2,1)} %param.40, bf16[512,2048]{1,0:T(8,128)(2,1)} %bitcast.53, bf16[1,2048,384]{2,1,0:T(8,128)(2,1)} %param.39, f32[512,384]{1,0:T(8,128)} %fusion.3), kind=kOutput, calls=%fused_computation.2 | convolution fusion | flops 1612840960 | bytes 8126464 | tf_op jit(solution)/shard_map/dot_general | solution.py:75
  100.5 3.8 %all-to-all-start.1 = ((bf16[32,16,2048]{2,1,0:T(8,128)(2,1)}), bf16[32,16,2048]{2,1,0:T(8,128)(2,1)}, u32[]{:S(2)}, u32[]{:S(2)}) async-start(bf16[32,16,2048]{2,1,0:T(8,128)(2,1)} %bitcast.51), calls=%async_computation.1 | async-start | bytes 4194304 | tf_op jit(solution)/shard_map/all_to_all | solution.py:153
  104.3 0.1 reduce_sum.77
  104.4 0.1 copy.44
  104.5 0.1 fusion.47
  104.7 48.3 %all-to-all-done.1 = bf16[32,16,2048]{2,1,0:T(8,128)(2,1)} async-done(((bf16[32,16,2048]{2,1,0:T(8,128)(2,1)}), bf16[32,16,2048]{2,1,0:T(8,128)(2,1)}, u32[]{:S(2)}, u32[]{:S(2)}) %all-to-all-start.1) | async-done | bytes 2097184 | tf_op jit(solution)/shard_map/all_to_all | solution.py:153
  153.0 2.1 %convert_reduce_fusion = f32[8,16,2048]{2,1,0:T(8,128)S(1)} fusion(bf16[32,16,2048]{2,1,0:T(8,128)(2,1)} %all-to-all-done.1), kind=kLoop, calls=%fused_computation.1 | loop fusion | flops 1835008 | bytes 3145728 | tf_op jit(solution)/shard_map/reduce_sum | solution.py:154
  155.1 0.7 convolution_reduce_fusion
  155.8 0.1 multiply_reduce_fusion
  155.9 0.8 fusion.27
  (64 shorter events, 0.3 us)
Async XLA Ops:
  0.6 28.7 %copy-start = (bf16[768,2048]{1,0:T(8,128)(2,1)S(1)}, bf16[768,2048]{1,0:T(8,128)(2,1)}, u32[]{:S(2)}) copy-start(bf16[768,2048]{1,0:T(8,128)(2,1)} %param.33) | copy-start | bytes 9437188
  0.6 3.4 %copy-start.2 = (bf16[32,2048]{1,0:T(8,128)(2,1)S(1)}, bf16[32,2048]{1,0:T(8,128)(2,1)}, u32[]{:S(2)}) copy-start(bf16[32,2048]{1,0:T(8,128)(2,1)} %param.21) | copy-start | bytes 393220
  0.7 3.4 %copy-start.6 = (f32[2048]{0:T(1024)S(1)}, f32[2048]{0:T(1024)}, u32[]{:S(2)}) copy-start(f32[2048]{0:T(1024)} %param.22) | copy-start | bytes 24580
  0.7 3.4 %copy-start.26 = (f32[4]{0:T(128)S(1)}, f32[4]{0:T(128)}, u32[]{:S(2)}) copy-start(f32[4]{0:T(128)} %param.28) | copy-start | bytes 52
  0.7 3.4 %copy-start.23 = (bf16[2048,4]{0,1:T(4,128)(2,1)S(1)}, bf16[2048,4]{0,1:T(4,128)(2,1)}, u32[]{:S(2)}) copy-start(bf16[2048,4]{0,1:T(4,128)(2,1)} %param.26) | copy-start | bytes 49156
  0.7 3.6 %copy-start.25 = (f32[32,4]{0,1:T(4,128)S(1)}, f32[32,4]{0,1:T(4,128)}, u32[]{:S(2)}) copy-start(f32[32,4]{0,1:T(4,128)} %param.32) | copy-start | bytes 1540
  0.7 3.6 %copy-start.27 = (f32[4]{0:T(128)S(1)}, f32[4]{0:T(128)}, u32[]{:S(2)}) copy-start(f32[4]{0:T(128)} %param.29) | copy-start | bytes 52
  0.7 3.6 %copy-start.24 = (bf16[2048,4]{0,1:T(4,128)(2,1)S(1)}, bf16[2048,4]{0,1:T(4,128)(2,1)}, u32[]{:S(2)}) copy-start(bf16[2048,4]{0,1:T(4,128)(2,1)} %param.27) | copy-start | bytes 49156
  1.9 4.4 %copy-start.17 = (f32[32]{0:T(128)}, f32[32]{0:T(128)S(1)}, u32[]{:S(2)}) copy-start(f32[32]{0:T(128)S(1)} %add_rsqrt_fusion.3) | copy-start | bytes 388
  4.6 0.6 copy-start.15
  5.3 9.1 %copy-start.5 = (f32[32,4]{1,0:T(8,128)}, f32[32,4]{1,0:T(8,128)S(1)}, u32[]{:S(2)}) copy-start(f32[32,4]{1,0:T(8,128)S(1)} %copy.39) | copy-start | bytes 1540
  6.1 2.0 %copy-start.10 = (s32[32,2]{0,1:T(2,128)}, s32[32,2]{0,1:T(2,128)S(1)}, u32[]{:S(2)}) copy-start(s32[32,2]{0,1:T(2,128)S(1)} %constant_dynamic-slice_fusion) | copy-start | bytes 772
  6.3 1.8 %copy-start.18 = (s32[64]{0:T(128)}, s32[64]{0:T(128)S(1)}, u32[]{:S(2)}) copy-start(s32[64]{0:T(128)S(1)} %eq.61) | copy-start | bytes 772
  9.1 2.0 %copy-start.19 = (s32[64]{0:T(128)}, s32[64]{0:T(128)S(1)}, u32[]{:S(2)}) copy-start(s32[64]{0:T(128)S(1)} %select_reduce_fusion) | copy-start | bytes 772
  9.2 6.1 %copy-start.16 = (f32[32,4]{0,1:T(4,128)S(1)}, f32[32,4]{0,1:T(4,128)}, u32[]{:S(2)}) copy-start(f32[32,4]{0,1:T(4,128)} %copy-done.15) | copy-start | bytes 1540
  11.1 3.3 %copy-start.4 = (f32[32,4,96]{2,1,0:T(4,128)S(1)}, f32[32,4,96]{2,1,0:T(4,128)}, u32[]{:S(2)}) copy-start(f32[32,4,96]{2,1,0:T(4,128)} %reshape.145) | copy-start | bytes 147460
  11.1 3.3 %copy-start.7 = (f32[32,4,96]{2,1,0:T(4,128)S(1)}, f32[32,4,96]{2,1,0:T(4,128)}, u32[]{:S(2)}) copy-start(f32[32,4,96]{2,1,0:T(4,128)} %param.31) | copy-start | bytes 147460
  23.0 6.1 %copy-start.1 = (f32[32,4,96,192]{3,2,1,0:T(8,128)}, f32[32,4,96,192]{3,2,1,0:T(8,128)S(1)}, u32[]{:S(2)}) copy-start(f32[32,4,96,192]{3,2,1,0:T(8,128)S(1)} %multiply_add_fusion) | copy-start | bytes 28311556
  23.0 6.1 %copy-start.8 = (f32[32,4]{1,0:T(8,128)S(1)}, f32[32,4]{1,0:T(8,128)}, u32[]{:S(2)}) copy-start(f32[32,4]{1,0:T(8,128)} %copy.42) | copy-start | bytes 1540
  29.1 1.0 copy-start.12
  29.3 1.2 copy-start.14
  29.4 3.7 %copy-start.21 = (s32[64]{0:T(128)S(1)}, s32[64]{0:T(128)}, u32[]{:S(2)}) copy-start(s32[64]{0:T(128)} %multiply_add_fusion.3) | copy-start | bytes 772
  34.7 57.1 %copy-start.22 = (bf16[1,2048,384]{2,1,0:T(8,128)(2,1)S(1)}, bf16[1,2048,384]{2,1,0:T(8,128)(2,1)}, u32[]{:S(2)}) copy-start(bf16[1,2048,384]{2,1,0:T(8,128)(2,1)} %param.38) | copy-start | bytes 4718596
  90.6 1.3 copy-start.3
  100.4 3.8 %copy-start.20 = (s32[64]{0:T(128)S(1)}, s32[64]{0:T(128)}, u32[]{:S(2)}) copy-start(s32[64]{0:T(128)} %copy-done.19) | copy-start | bytes 772
  100.4 4.0 %copy-start.9 = (bf16[2048,8]{0,1:T(8,128)(2,1)S(1)}, bf16[2048,8]{0,1:T(8,128)(2,1)}, u32[]{:S(2)}) copy-start(bf16[2048,8]{0,1:T(8,128)(2,1)} %param.36) | copy-start | bytes 98308
  100.5 4.2 %copy-start.11 = (s32[32,2]{0,1:T(2,128)S(1)}, s32[32,2]{0,1:T(2,128)}, u32[]{:S(2)}) copy-start(s32[32,2]{0,1:T(2,128)} %copy-done.10) | copy-start | bytes 772
  100.5 52.5 %all-to-all-start.1 = ((bf16[32,16,2048]{2,1,0:T(8,128)(2,1)}), bf16[32,16,2048]{2,1,0:T(8,128)(2,1)}, u32[]{:S(2)}, u32[]{:S(2)}) async-start(bf16[32,16,2048]{2,1,0:T(8,128)(2,1)} %bitcast.51), calls=%async_computation.1 | async-start | bytes 4194304 | tf_op jit(solution)/shard_map/all_to_all | solution.py:153
  104.7 51.2 %copy-start.13 = (f32[2048]{0:T(1024)S(1)}, f32[2048]{0:T(1024)}, u32[]{:S(2)}) copy-start(f32[2048]{0:T(1024)} %param.41) | copy-start | bytes 24580
where the time goes:
time: 157 us
  blocking collectives  55.8 us (36%)
  waiting for transfers between devices  48.3 us (31%)
  matrix products  25 us (16%)
  other arithmetic  13.8 us (9%)
  local copies, waits for them, and re-layouts  8.9 us (6%)
  starting transfers between devices  3.79 us (2%)
    all_to_all x1, blocking collectives, body(): lax.all_to_all(outgoing, 'ep', split_axis=0, concat_axis=0, tiled=True)  55.8 us
    all_to_all x1, waiting for transfers between devices, body(): lax.all_to_all(computed, 'ep', split_axis=0, concat_axis=0, tiled=True)  48.3 us
    dot_general x1, matrix products, expert_quarter(): jnp.dot(hidden, down_w, preferred_element_type=jnp.float32)  6.43 us
    add x1, other arithmetic, cell_step(): keep_weight[:, :, None, None] * memory_cells  6.1 us
    dot_general x1, matrix products, cell_step(): jnp.einsum('bhd,bhde->bhe', query_rows, cells_next, precision=lax.Precisi...  6.1 us
    all_to_all x1, starting transfers between devices, body(): lax.all_to_all(computed, 'ep', split_axis=0, concat_axis=0, tiled=True)  3.79 us
    dot_general x1, matrix products, cell_step(): jnp.dot(normed, w_value, preferred_element_type=jnp.float32)  3.24 us
  transfers between devices with their start and end apart: 1, of which 1 were waited for; matrix products, arithmetic and copies ran while one was open for 0% of the time, Pallas kernels for 0%

commit v1 on v0

--- a/solution.py
+++ b/solution.py
@@ -1,6 +1,10 @@
+import functools
+
 import jax
 import jax.numpy as jnp
 from jax import lax
+from jax.experimental import pallas as pl
+from jax.experimental.pallas import tpu as pltpu
 from jax.sharding import PartitionSpec as P
 
 epsilon = 1e-06
@@ -73,6 +77,211 @@
     up_part = jnp.dot(row_block, up_w, preferred_element_type=jnp.float32)
     hidden = (jax.nn.silu(gate_part) * up_part).astype(jnp.bfloat16)
     return jnp.dot(hidden, down_w, preferred_element_type=jnp.float32).astype(jnp.bfloat16)
+
+
+VMEM = pl.BlockSpec(memory_space=pltpu.VMEM)
+
+
+def remote_copy(src, dst, sems, kind, step, target):
+    return pltpu.make_async_remote_copy(
+        src_ref=src,
+        dst_ref=dst,
+        send_sem=sems[0].at[kind, step],
+        recv_sem=sems[1].at[kind, step],
+        device_id=(target,),
+        device_id_type=pl.DeviceIdType.MESH,
+    )
+
+
+def places(group_size):
+    me = lax.axis_index("ep")
+    own = lax.div(me, group_size)
+    member = lax.rem(me, group_size)
+    core_mate = member + 1 - 2 * lax.rem(member, 2)
+    chip_mate = lax.rem(member + 2, group_size)
+    far_mate = lax.rem(core_mate + 2, group_size)
+    return own, member, core_mate, chip_mate, far_mate
+
+
+def greet(experts, group_size):
+    own, member, core_mate, chip_mate, _ = places(group_size)
+    barrier = pltpu.get_barrier_semaphore()
+
+    def signal(target):
+        pl.semaphore_signal(
+            barrier, inc=1, device_id=(target,), device_id_type=pl.DeviceIdType.MESH
+        )
+
+    for step in range(1, experts):
+        signal(lax.rem(own + step, experts) * group_size + member)
+    signal(own * group_size + core_mate)
+    signal(own * group_size + chip_mate)
+    pl.semaphore_wait(barrier, experts + 1)
+
+
+def dispatch_kernel(experts, group_size, outgoing, arrived, send_sems, recv_sems):
+    own, member, core_mate, chip_mate, _ = places(group_size)
+    sems = (send_sems, recv_sems)
+    greet(experts, group_size)
+
+    def direct(step):
+        target = lax.rem(own + step, experts)
+        return remote_copy(
+            outgoing.at[target],
+            arrived.at[own, member],
+            sems,
+            0,
+            step,
+            target * group_size + member,
+        )
+
+    def forward(step, kind):
+        source = lax.rem(own + experts - step, experts)
+        mate = core_mate if kind != 2 else chip_mate
+        row = member if kind != 3 else chip_mate
+        src = arrived.at[source, row]
+        if step == 0 and kind != 3:
+            src = outgoing.at[own]
+        return remote_copy(
+            src, arrived.at[source, row], sems, kind, step, own * group_size + mate
+        )
+
+    for step in range(1, experts):
+        direct(step).start()
+    forward(0, 2).start()
+    forward(0, 1).start()
+    arrived[own, member] = outgoing[own]
+    for step in range(1, experts):
+        direct(step).wait_recv()
+        forward(step, 2).start()
+        forward(step, 1).start()
+        forward(step - 1, 2).wait_recv()
+        forward(step - 1, 3).start()
+    forward(experts - 1, 2).wait_recv()
+    forward(experts - 1, 3).start()
+    for step in range(experts):
+        if step:
+            direct(step).wait_send()
+        forward(step, 2).wait_send()
+        forward(step, 1).wait()
+        forward(step, 3).wait()
+
+
+def dispatch_rows(outgoing, group_size):
+    experts, capacity, width = outgoing.shape
+    return pl.pallas_call(
+        functools.partial(dispatch_kernel, experts, group_size),
+        out_shape=jax.ShapeDtypeStruct((experts, group_size, capacity, width), outgoing.dtype),
+        in_specs=[VMEM],
+        out_specs=VMEM,
+        scratch_shapes=[
+            pltpu.SemaphoreType.DMA((4, experts)),
+            pltpu.SemaphoreType.DMA((4, experts)),
+        ],
+        compiler_params=pltpu.CompilerParams(collective_id=0, has_side_effects=True),
+        name="dispatch_rows",
+    )(outgoing)
+
+
+def return_kernel(
+    experts,
+    group_size,
+    computed,
+    returned,
+    core_in,
+    chip_out,
+    chip_in,
+    final_out,
+    send_sems,
+    recv_sems,
+):
+    own, member, core_mate, chip_mate, far_mate = places(group_size)
+    sems = (send_sems, recv_sems)
+    greet(experts, group_size)
+
+    def source_of(step):
+        return lax.rem(own + step, experts)
+
+    def to_core(step, kind):
+        row = core_mate if kind == 0 else far_mate
+        return remote_copy(
+            computed.at[source_of(step), row],
+            core_in.at[kind, step],
+            sems,
+            kind,
+            step,
+            own * group_size + core_mate,
+        )
+
+    def to_chip(step):
+        return remote_copy(
+            chip_out.at[step], chip_in.at[step], sems, 2, step, own * group_size + chip_mate
+        )
+
+    def to_source(step):
+        target = source_of(step)
+        return remote_copy(
+            final_out.at[step], returned.at[own], sems, 3, step, target * group_size + member
+        )
+
+    def wide(values):
+        return values.astype(jnp.float32)
+
+    order = list(range(1, experts)) + [0]
+    for step in order:
+        to_core(step, 1).start()
+        to_core(step, 0).start()
+    before = None
+    for step in order:
+        to_core(step, 1).wait_recv()
+        total = wide(computed[source_of(step), chip_mate]) + wide(core_in[1, step])
+        chip_out[step] = total.astype(chip_out.dtype)
+        if before is not None:
+            to_chip(before).start()
+        before = step
+    for step in order:
+        to_core(step, 0).wait_recv()
+        if before is not None:
+            to_chip(before).start()
+            before = None
+    for step in order:
+        to_chip(step).wait_recv()
+        total = wide(computed[source_of(step), member]) + wide(core_in[0, step])
+        total = (total + wide(chip_in[step])).astype(final_out.dtype)
+        if step:
+            final_out[step] = total
+        else:
+            returned[own] = total
+        if before is not None:
+            to_source(before).start()
+        before = step if step else None
+    for step in range(experts):
+        to_core(step, 0).wait_send()
+        to_core(step, 1).wait_send()
+        to_chip(step).wait_send()
+        if step:
+            to_source(step).wait()
+
+
+def return_rows(computed):
+    experts, group_size, capacity, width = computed.shape
+    chunk = (experts, capacity, width)
+    return pl.pallas_call(
+        functools.partial(return_kernel, experts, group_size),
+        out_shape=jax.ShapeDtypeStruct(chunk, computed.dtype),
+        in_specs=[VMEM],
+        out_specs=VMEM,
+        scratch_shapes=[
+            pltpu.VMEM((2,) + chunk, computed.dtype),
+            pltpu.VMEM(chunk, computed.dtype),
+            pltpu.VMEM(chunk, computed.dtype),
+            pltpu.VMEM(chunk, computed.dtype),
+            pltpu.SemaphoreType.DMA((4, experts)),
+            pltpu.SemaphoreType.DMA((4, experts)),
+        ],
+        compiler_params=pltpu.CompilerParams(collective_id=1, has_side_effects=True),
+        name="return_rows",
+    )(computed)
 
 
 def body(
@@ -135,29 +344,18 @@
         jnp.int32
     )
     slot_index = jnp.sum((jnp.cumsum(flat_hot, axis=0) - 1) * flat_hot, axis=1)
-    position = flat_routes * capacity + slot_index
-    dispatch = position[:, None] == jnp.arange(experts * capacity, dtype=jnp.int32)[None, :]
-    repeated = jnp.repeat(expert_in, top_count, axis=0)
+    position = (flat_routes * capacity + slot_index).reshape(seq_rows, top_count)
+    placed = position[:, :, None] == jnp.arange(experts * capacity, dtype=jnp.int32)
+    dispatch = jnp.any(placed, axis=1).astype(jnp.bfloat16)
     outgoing = jnp.einsum(
-        "rp,rd->pd", dispatch.astype(jnp.bfloat16), repeated, preferred_element_type=jnp.float32
+        "rp,rd->pd", dispatch, expert_in, preferred_element_type=jnp.float32
     ).astype(jnp.bfloat16)
-    outgoing = jnp.broadcast_to(
-        outgoing.reshape(experts, 1, capacity, model_width),
-        (experts, group_size, capacity, model_width),
-    ).reshape(devices, capacity, model_width)
-    arrived = lax.all_to_all(outgoing, "ep", split_axis=0, concat_axis=0, tiled=True)
-    shape_in = arrived.shape
-    computed = expert_quarter(arrived.reshape(-1, model_width), gate_w, up_w, down_w).reshape(
-        shape_in
-    )
-    returned = lax.all_to_all(computed, "ep", split_axis=0, concat_axis=0, tiled=True)
-    summed = jnp.sum(
-        returned.astype(jnp.float32).reshape(experts, group_size, capacity, model_width), axis=1
-    )
-    summed = summed.reshape(experts * capacity, model_width)
-    combine = jnp.where(dispatch, route_weight.reshape(-1)[:, None], 0.0)
-    expert_rows = jnp.dot(combine, summed, precision=lax.Precision.HIGHEST)
-    expert_sum = jnp.sum(expert_rows.reshape(seq_rows, top_count, model_width), axis=1)
+    arrived = dispatch_rows(outgoing.reshape(experts, capacity, model_width), group_size)
+    computed = expert_quarter(arrived.reshape(-1, model_width), gate_w, up_w, down_w)
+    returned = return_rows(computed.reshape(arrived.shape))
+    summed = returned.astype(jnp.float32).reshape(experts * capacity, model_width)
+    combine = jnp.sum(jnp.where(placed, route_weight[:, :, None], 0.0), axis=1)
+    expert_sum = jnp.dot(combine, summed, precision=lax.Precision.HIGHEST)
     mixed = (after_float + normalize(expert_sum, gain_ffn_post)).astype(jnp.bfloat16)
     return (mixed, cells_next, norm_next, stab_next)
 

time: 157 us -> 108 us (0.69)
  Pallas kernels: 0 us -> 55.9 us
  blocking collectives: 55.8 us -> 0 us
  waiting for transfers between devices: 48.3 us -> 0 us
  matrix products: 25 us -> 32.4 us
  local copies, waits for them, and re-layouts: 8.9 us -> 3.5 us
  starting transfers between devices: 3.79 us -> 0 us
    pallas_call x0 -> x2, Pallas kernels: none -> 55.9 us  [the longest x1 29.2 us: dispatch_rows(): pl.pallas_call(functools.partial(dispatch_kernel, experts, group_size), o...]
    all_to_all x1 -> x0, blocking collectives: 55.8 us -> none  [body(): lax.all_to_all(outgoing, 'ep', split_axis=0, concat_axis=0, tiled=True)]
    all_to_all x1 -> x0, waiting for transfers between devices: 48.3 us -> none  [body(): lax.all_to_all(computed, 'ep', split_axis=0, concat_axis=0, tiled=True)]
    add x1, other arithmetic: 6.1 us -> 9.94 us  [cell_step(): keep_weight[:, :, None, None] * memory_cells]
    all_to_all x1 -> x0, starting transfers between devices: 3.79 us -> none  [body(): lax.all_to_all(computed, 'ep', split_axis=0, concat_axis=0, tiled=True)]
    dot_general x1, matrix products: 6.1 us -> 8.97 us  [cell_step(): jnp.einsum('bhd,bhde->bhe', query_rows, cells_next, precision=lax.Precisi...]
    dot_general x1, matrix products: 2.14 us -> 4.17 us  [expert_quarter(): gate_part = jnp.dot(row_block, gate_w, preferred_element_type=jnp.float32)]
    reduce_sum x1, other arithmetic: 2.12 us -> 0.09 us  [body(): combine = jnp.sum(jnp.where(placed, route_weight[:, :, None], 0.0), axis=1)]
  transfers between devices with their start and end apart: 1 -> 0, of which waited for: 1 -> 0; matrix products, arithmetic and copies ran while one was open for 0% -> 0% of each run, Pallas kernels for 0% -> 0%
where the time goes in v1:
time: 108 us
  Pallas kernels  55.9 us (52%)
  matrix products  32.4 us (30%)
  other arithmetic  15.1 us (14%)
  local copies, waits for them, and re-layouts  3.5 us (3%)
    pallas_call x1, Pallas kernels, dispatch_rows(): pl.pallas_call(functools.partial(dispatch_kernel, experts, group_size), o...  29.2 us
    pallas_call x1, Pallas kernels, return_rows(): pl.pallas_call(functools.partial(return_kernel, experts, group_size), out...  26.7 us
    add x1, other arithmetic, cell_step(): keep_weight[:, :, None, None] * memory_cells  9.94 us
    dot_general x1, matrix products, cell_step(): jnp.einsum('bhd,bhde->bhe', query_rows, cells_next, precision=lax.Precisi...  8.97 us
    dot_general x1, matrix products, expert_quarter(): jnp.dot(hidden, down_w, preferred_element_type=jnp.float32)  6.39 us
    dot_general x1, matrix products, expert_quarter(): gate_part = jnp.dot(row_block, gate_w, preferred_element_type=jnp.float32)  4.17 us
    dot_general x1, matrix products, cell_step(): jnp.dot(normed, w_value, preferred_element_type=jnp.float32)  3.2 us
    unnamed x1, other arithmetic  2.2 us

profile of v1, /device:TPU:0, one launch (start us, length us, event | category | flops | bytes accessed | tf_op | source)
XLA Modules:
  0.0 107.8 jit_solution(15321088990239031925)
XLA Ops:
  0.6 0.0 copy-start
  0.6 0.0 copy-start.1
  0.7 0.0 copy-start.2
  0.7 1.2 %fusion.20 = f32[32]{0:T(128)S(1)} fusion(bf16[32,2048]{1,0:T(8,128)(2,1)} %param.21), kind=kLoop, calls=%fused_computation.28 | loop fusion | flops 196576 | bytes 131200 | tf_op jit(solution)/shard_map/reduce_sum | solution.py:14
  1.9 1.2 %convolution_add_fusion = f32[32,4]{0,1:T(4,128)S(1)} fusion(bf16[2048,4]{0,1:T(4,128)(2,1)} %param.26, f32[4]{0:T(128)} %param.28, bf16[32,2048]{1,0:T(8,128)(2,1)} %param.21, f32[2048]{0:T(1024)} %param.22, f32[32]{0:T(128)S(1)} %add_rsqrt_fusion.3), kind=kOutput, calls=%fused_computation.13 | convolution fusion | flops 786560 | bytes 156304 | tf_op jit(solution)/shard_map/dot_general | solution.py:43
  3.0 1.2 %subtract_exponential_fusion.1 = (f32[32,4]{0,1:T(4,128)S(1)}, f32[32,4]{0,1:T(4,128)S(1)}) fusion(f32[32,4]{0,1:T(4,128)S(1)} %convolution_add_fusion, f32[32,4]{0,1:T(4,128)} %param.32, f32[4]{0:T(128)} %param.29, bf16[2048,4]{0,1:T(4,128)(2,1)} %param.27, bf16[32,2048]{1,0:T(8,128)(2,1)} %param.21, f32[2048]{0:T(1024)} %param.22, f32[32]{0:T(128)S(1)} %add_rsqrt_fusion.3), kind=kOutput, calls=%fused_computation.59 | convolution fusion | flops 787968 | bytes 157840 | tf_op jit(solution)/shard_map/dot_general | solution.py:45
  4.2 0.0 copy-start.7
  4.2 0.7 copy.38
  4.9 0.1 copy.37
  5.0 1.9 %convolution_convert_fusion.4 = bf16[32,384]{1,0:T(8,128)(2,1)S(1)} fusion(bf16[2048,384]{1,0:T(8,128)(2,1)} %param.23, bf16[32,2048]{1,0:T(8,128)(2,1)} %param.21, f32[2048]{0:T(1024)} %param.22, f32[32]{0:T(128)S(1)} %add_rsqrt_fusion.3), kind=kOutput, calls=%fused_computation.12 | convolution fusion | flops 50606080 | bytes 1736832 | tf_op jit(solution)/shard_map/dot_general | solution.py:35
  6.9 0.1 mul.159
  7.0 0.0 copy-done.1
  7.0 0.0 copy-done.2
  7.1 1.8 %convolution_convert_fusion.3 = bf16[32,384]{1,0:T(8,128)(2,1)S(1)} fusion(bf16[2048,384]{1,0:T(8,128)(2,1)} %param.24, bf16[32,2048]{1,0:T(8,128)(2,1)S(1)} %copy-done.1, f32[2048]{0:T(1024)S(1)} %copy-done.2, f32[32]{0:T(128)S(1)} %add_rsqrt_fusion.3), kind=kOutput, calls=%fused_computation.11 | convolution fusion | flops 50606080 | bytes 1736832 | tf_op jit(solution)/shard_map/dot_general | solution.py:37
  8.9 0.1 reshape.97
  9.0 2.2 %multiply_reduce_fusion.2 = (f32[32,4]{1,0:T(8,128)}, f32[32,4,96]{2,1,0:T(4,128)}, f32[32,4,96]{2,1,0:T(4,128)S(1)}) fusion(f32[32,4,96]{2,1,0:T(4,128)S(1)} %mul.159, f32[32,4,96]{2,1,0:T(4,128)} %param.31, f32[32,4]{1,0:T(8,128)S(1)} %copy.37, f32[32,4,96]{2,1,0:T(4,128)S(1)} %reshape.97, f32[32,4]{1,0:T(8,128)} %copy.38), kind=kLoop, calls=%fused_computation.40 | loop fusion | flops 61312 | bytes 247296
  11.2 3.2 %convolution_convert_fusion.2 = bf16[32,768]{1,0:T(8,128)(2,1)} fusion(bf16[2048,768]{1,0:T(8,128)(2,1)} %param.25, bf16[32,2048]{1,0:T(8,128)(2,1)S(1)} %copy-done.1, f32[2048]{0:T(1024)S(1)} %copy-done.2, f32[32]{0:T(128)S(1)} %add_rsqrt_fusion.3), kind=kOutput, calls=%fused_computation.10 | convolution fusion | flops 100950016 | bytes 3334272 | tf_op jit(solution)/shard_map/dot_general | solution.py:40
  14.4 0.9 reshape.98
  15.3 9.9 %multiply_add_fusion = f32[32,4,96,192]{3,2,1,0:T(8,128)} fusion(f32[32,4,96,192]{3,2,1,0:T(8,128)} %param.30, f32[32,4,192]{2,1,0:T(4,128)S(1)} %reshape.98, f32[32,4,96]{2,1,0:T(4,128)S(1)} %get-tuple-element.8, f32[32,4]{1,0:T(8,128)S(1)} %copy.37), kind=kLoop, calls=%fused_computation | loop fusion | flops 7077888 | bytes 19022336 | tf_op jit(solution)/shard_map/add | solution.py:53
  25.3 0.1 reshape.99
  25.4 9.0 %fusion.43 = f32[32,4,1,192]{3,2,1,0:T(1,128)S(1)} fusion(f32[32,4,96,1]{2,3,1,0:T(1,128)S(1)} %bitcast.44, f32[32,4,96,192]{3,2,1,0:T(8,128)} %multiply_add_fusion), kind=kOutput, calls=%fused_computation.67 | convolution fusion | flops 28311552 | bytes 9584640 | tf_op jit(solution)/shard_map/bhd,bhde->bhe/dot_general | solution.py:57
  34.3 0.0 copy-start.4
  34.4 0.1 copy.49
  34.5 0.1 copy.40
  34.5 0.1 fusion.28
  34.7 0.1 convert_element_type.59
  34.8 0.0 copy-start.5
  34.8 0.7 multiply_reduce_fusion.1
  35.6 0.2 fusion.24
  35.8 0.8 constant_dynamic-slice_fusion
  36.6 0.1 copy.50
  36.7 0.1 eq.20
  36.8 0.1 fusion.33
  36.8 0.1 reduce_window_sum.11
  36.9 0.2 select_reduce_fusion.1
  37.1 0.1 reduce_sum.68
  37.3 0.1 copy.42
  37.3 0.1 fusion.32
  37.4 0.0 copy-done.5
  37.4 1.2 %convolution_convert_fusion.1 = bf16[128,2048]{1,0:T(8,128)(2,1)} fusion(pred[32,128]{1,0:T(8,128)(4,1)S(1)} %fusion.32, bf16[32,2048]{1,0:T(8,128)(2,1)S(1)} %get-tuple-element.5, f32[2048]{0:T(1024)S(1)} %copy-done.5, f32[32]{0:T(128)S(1)} %add_rsqrt_fusion.1), kind=kOutput, calls=%fused_computation.2 | convolution fusion | flops 17301504 | bytes 667776 | tf_op jit(solution)/shard_map/rp,rd->pd/dot_general | solution.py:350
  38.6 29.2 %dispatch_rows.1 = bf16[8,4,16,2048]{3,2,1,0:T(8,128)(2,1)} custom-call(bf16[8,16,2048]{2,1,0:T(8,128)(2,1)} %bitcast.43), custom_call_target="tpu_custom_call" | custom-call | tf_op jit(solution)/shard_map/dispatch_rows/pallas_call | solution.py:172
  67.8 4.2 %fusion.3 = f32[512,384]{1,0:T(8,128)} fusion(bf16[512,2048]{1,0:T(8,128)(2,1)} %bitcast.39, bf16[1,2048,384]{2,1,0:T(8,128)(2,1)} %param.38), kind=kOutput, calls=%fused_computation.6 | convolution fusion | flops 805306368 | bytes 4456448 | tf_op jit(solution)/shard_map/dot_general | solution.py:76
  72.0 6.4 %convolution_convert_fusion = bf16[512,2048]{1,0:T(8,128)(2,1)} fusion(bf16[1,384,2048]{2,1,0:T(8,128)(2,1)} %param.40, bf16[512,2048]{1,0:T(8,128)(2,1)} %bitcast.40, bf16[1,2048,384]{2,1,0:T(8,128)(2,1)} %param.39, f32[512,384]{1,0:T(8,128)} %fusion.3), kind=kOutput, calls=%fused_computation.1 | convolution fusion | flops 1612840960 | bytes 8126464 | tf_op jit(solution)/shard_map/dot_general | solution.py:79
  78.4 26.7 %return_rows.1 = bf16[8,16,2048]{2,1,0:T(8,128)(2,1)} custom-call(bf16[8,4,16,2048]{3,2,1,0:T(8,128)(2,1)} %bitcast.41), custom_call_target="tpu_custom_call" | custom-call | tf_op jit(solution)/shard_map/return_rows/pallas_call | solution.py:269
  105.1 0.2 fusion.30
  105.4 0.1 select_reduce_fusion
  105.5 1.5 %multiply_reduce_fusion = (f32[32]{0:T(128)S(1)}, f32[32,2048]{1,0:T(8,128)S(1)}) fusion(f32[32,128]{1,0:T(8,128)S(1)} %select_reduce_fusion, bf16[128,2048]{1,0:T(8,128)(2,1)} %bitcast.42), kind=kOutput, calls=%fused_computation.36 | convolution fusion | flops 100794336 | bytes 802944 | tf_op jit(solution)/shard_map/dot_general | solution.py:358
  107.0 0.8 fusion.27
  (20 shorter events, 0.1 us)
Async XLA Ops:
  0.6 34.1 %copy-start = (bf16[768,2048]{1,0:T(8,128)(2,1)S(1)}, bf16[768,2048]{1,0:T(8,128)(2,1)}, u32[]{:S(2)}) copy-start(bf16[768,2048]{1,0:T(8,128)(2,1)} %param.33) | copy-start | bytes 9437188
  0.6 6.4 %copy-start.1 = (bf16[32,2048]{1,0:T(8,128)(2,1)S(1)}, bf16[32,2048]{1,0:T(8,128)(2,1)}, u32[]{:S(2)}) copy-start(bf16[32,2048]{1,0:T(8,128)(2,1)} %param.21) | copy-start | bytes 393220
  0.7 6.4 %copy-start.2 = (f32[2048]{0:T(1024)S(1)}, f32[2048]{0:T(1024)}, u32[]{:S(2)}) copy-start(f32[2048]{0:T(1024)} %param.22) | copy-start | bytes 24580
  4.2 30.2 %copy-start.7 = (f32[32,4]{0,1:T(4,128)}, f32[32,4]{0,1:T(4,128)S(1)}, u32[]{:S(2)}) copy-start(f32[32,4]{0,1:T(4,128)S(1)} %get-tuple-element.10) | copy-start | bytes 1540
  25.4 9.0 %copy-start.3 = (f32[32,4]{1,0:T(8,128)S(1)}, f32[32,4]{1,0:T(8,128)}, u32[]{:S(2)}) copy-start(f32[32,4]{1,0:T(8,128)} %get-tuple-element.6) | copy-start | bytes 1540
  34.3 1.2 %copy-start.4 = (f32[2048]{0:T(1024)S(1)}, f32[2048]{0:T(1024)}, u32[]{:S(2)}) copy-start(f32[2048]{0:T(1024)} %param.34) | copy-start | bytes 24580
  34.8 2.6 %copy-start.5 = (f32[2048]{0:T(1024)S(1)}, f32[2048]{0:T(1024)}, u32[]{:S(2)}) copy-start(f32[2048]{0:T(1024)} %param.35) | copy-start | bytes 24580
  78.4 26.7 %copy-start.8 = (bf16[2048,8]{0,1:T(8,128)(2,1)S(1)}, bf16[2048,8]{0,1:T(8,128)(2,1)}, u32[]{:S(2)}) copy-start(bf16[2048,8]{0,1:T(8,128)(2,1)} %param.36) | copy-start | bytes 98308
  78.4 28.6 %copy-start.6 = (f32[2048]{0:T(1024)S(1)}, f32[2048]{0:T(1024)}, u32[]{:S(2)}) copy-start(f32[2048]{0:T(1024)} %param.41) | copy-start | bytes 24580

commit v2 on v1

--- a/solution.py
+++ b/solution.py
@@ -16,6 +16,53 @@
 
 def rounded(values):
     return lax.optimization_barrier(values.astype(jnp.bfloat16)).astype(jnp.float32)
+
+
+def cell_kernel(keep, cells, queries, keys, values, cells_next, numerator):
+    block, heads, key_size, value_size = cells.shape
+    first = pl.program_id(0) * block
+    for row in range(block):
+        for head in range(heads):
+            span = slice(head * key_size, (head + 1) * key_size)
+            key_column = keys[0, span, row : row + 1]
+            query_column = queries[0, span, row : row + 1]
+            value_row = values[row, head : head + 1, :]
+            updated = keep[first + row, head] * cells[row, head] + key_column * value_row
+            cells_next[row, head] = updated
+            numerator[row, head : head + 1, :] = jnp.sum(
+                query_column * updated, axis=0, keepdims=True
+            )
+
+
+def update_cells(keep, cells, queries, keys, values):
+    rows, heads, key_size, value_size = cells.shape
+    block = next(size for size in (4, 2, 1) if rows % size == 0)
+
+    def columns(array):
+        flat = array.reshape(rows // block, block, heads * key_size)
+        return jnp.swapaxes(flat, 1, 2)
+
+    cell_spec = pl.BlockSpec((block, heads, key_size, value_size), lambda i: (i, 0, 0, 0))
+    column_spec = pl.BlockSpec((1, heads * key_size, block), lambda i: (i, 0, 0))
+    value_spec = pl.BlockSpec((block, heads, value_size), lambda i: (i, 0, 0))
+    return pl.pallas_call(
+        cell_kernel,
+        grid=(rows // block,),
+        out_shape=(
+            jax.ShapeDtypeStruct(cells.shape, jnp.float32),
+            jax.ShapeDtypeStruct(values.shape, jnp.float32),
+        ),
+        in_specs=[
+            pl.BlockSpec(memory_space=pltpu.SMEM),
+            cell_spec,
+            column_spec,
+            column_spec,
+            value_spec,
+        ],
+        out_specs=(cell_spec, value_spec),
+        compiler_params=pltpu.CompilerParams(vmem_limit_bytes=16 * 2**20),
+        name="update_cells",
+    )(keep, cells, columns(queries), columns(keys), values)
 
 
 def cell_step(
@@ -49,12 +96,10 @@
     keep_weight = jnp.exp(carried - stab_next)
     write_weight = jnp.exp(input_gate - stab_next)
     scaled_keys = write_weight[:, :, None] * key_rows
-    cells_next = (
-        keep_weight[:, :, None, None] * memory_cells
-        + scaled_keys[:, :, :, None] * value_rows[:, :, None, :]
-    )
     norm_next = keep_weight[:, :, None] * normalizer + scaled_keys
-    numerator = jnp.einsum("bhd,bhde->bhe", query_rows, cells_next, precision=lax.Precision.HIGHEST)
+    cells_next, numerator = update_cells(
+        keep_weight, memory_cells, query_rows, scaled_keys, value_rows
+    )
     denominator = jnp.einsum("bhd,bhd->bh", query_rows, norm_next, precision=lax.Precision.HIGHEST)
     denominator = jnp.maximum(jnp.abs(denominator), jnp.exp(-stab_next))
     cell_out = (
@@ -70,13 +115,6 @@
     onehot = routes[:, :, None] == jnp.arange(w_router.shape[1], dtype=jnp.int32)[None, None, :]
     chosen = jnp.sum(jnp.where(onehot, logits[:, None, :], 0.0), axis=-1)
     return jax.nn.sigmoid(chosen - chosen[:, ::-1])
-
-
-def expert_quarter(row_block, gate_w, up_w, down_w):
-    gate_part = jnp.dot(row_block, gate_w, preferred_element_type=jnp.float32)
-    up_part = jnp.dot(row_block, up_w, preferred_element_type=jnp.float32)
-    hidden = (jax.nn.silu(gate_part) * up_part).astype(jnp.bfloat16)
-    return jnp.dot(hidden, down_w, preferred_element_type=jnp.float32).astype(jnp.bfloat16)
 
 
 VMEM = pl.BlockSpec(memory_space=pltpu.VMEM)
@@ -103,6 +141,16 @@
     return own, member, core_mate, chip_mate, far_mate
 
 
+def paired(own, step):
+    other = own
+    bit = 1
+    while bit <= step:
+        if step & bit:
+            other = other + bit - 2 * bit * lax.rem(lax.div(own, bit), 2)
+        bit *= 2
+    return other
+
+
 def greet(experts, group_size):
     own, member, core_mate, chip_mate, _ = places(group_size)
     barrier = pltpu.get_barrier_semaphore()
@@ -113,7 +161,7 @@
         )
 
     for step in range(1, experts):
-        signal(lax.rem(own + step, experts) * group_size + member)
+        signal(paired(own, step) * group_size + member)
     signal(own * group_size + core_mate)
     signal(own * group_size + chip_mate)
     pl.semaphore_wait(barrier, experts + 1)
@@ -125,7 +173,7 @@
     greet(experts, group_size)
 
     def direct(step):
-        target = lax.rem(own + step, experts)
+        target = paired(own, step)
         return remote_copy(
             outgoing.at[target],
             arrived.at[own, member],
@@ -136,7 +184,7 @@
         )
 
     def forward(step, kind):
-        source = lax.rem(own + experts - step, experts)
+        source = paired(own, step)
         mate = core_mate if kind != 2 else chip_mate
         row = member if kind != 3 else chip_mate
         src = arrived.at[source, row]
@@ -167,6 +215,31 @@
         forward(step, 3).wait()
 
 
+def expert_kernel(rows_in, gate_w, up_w, down_w, result):
+    rows = rows_in.shape[0]
+    pieces = 2 if rows % 512 == 0 else 1
+    for piece in range(pieces):
+        span = slice(piece * rows // pieces, (piece + 1) * rows // pieces)
+        block = rows_in[span, :]
+        gate_part = jnp.dot(block, gate_w[0], preferred_element_type=jnp.float32)
+        up_part = jnp.dot(block, up_w[0], preferred_element_type=jnp.float32)
+        hidden = (jax.nn.silu(gate_part) * up_part).astype(rows_in.dtype)
+        result[span, :] = jnp.dot(
+            hidden, down_w[0], preferred_element_type=jnp.float32
+        ).astype(result.dtype)
+
+
+def expert_quarter(rows_in, gate_w, up_w, down_w):
+    return pl.pallas_call(
+        expert_kernel,
+        out_shape=jax.ShapeDtypeStruct(rows_in.shape, rows_in.dtype),
+        in_specs=[VMEM] * 4,
+        out_specs=VMEM,
+        compiler_params=pltpu.CompilerParams(vmem_limit_bytes=24 * 2**20),
+        name="expert_quarter",
+    )(rows_in, gate_w, up_w, down_w)
+
+
 def dispatch_rows(outgoing, group_size):
     experts, capacity, width = outgoing.shape
     return pl.pallas_call(
@@ -178,7 +251,9 @@
             pltpu.SemaphoreType.DMA((4, experts)),
             pltpu.SemaphoreType.DMA((4, experts)),
         ],
-        compiler_params=pltpu.CompilerParams(collective_id=0, has_side_effects=True),
+        compiler_params=pltpu.CompilerParams(
+            collective_id=0, has_side_effects=True, vmem_limit_bytes=12 * 2**20
+        ),
         name="dispatch_rows",
     )(outgoing)
 
@@ -200,7 +275,7 @@
     greet(experts, group_size)
 
     def source_of(step):
-        return lax.rem(own + step, experts)
+        return paired(own, step)
 
     def to_core(step, kind):
         row = core_mate if kind == 0 else far_mate
@@ -227,7 +302,7 @@
     def wide(values):
         return values.astype(jnp.float32)
 
-    order = list(range(1, experts)) + [0]
+    order = list(range(experts - 1, -1, -1))
     for step in order:
         to_core(step, 1).start()
         to_core(step, 0).start()
@@ -279,7 +354,9 @@
             pltpu.SemaphoreType.DMA((4, experts)),
             pltpu.SemaphoreType.DMA((4, experts)),
         ],
-        compiler_params=pltpu.CompilerParams(collective_id=1, has_side_effects=True),
+        compiler_params=pltpu.CompilerParams(
+            collective_id=1, has_side_effects=True, vmem_limit_bytes=16 * 2**20
+        ),
         name="return_rows",
     )(computed)
 
@@ -334,9 +411,6 @@
     after_mix = (residual + normalize(mix_out, gain_mix_post)).astype(jnp.bfloat16)
     after_float = after_mix.astype(jnp.float32)
     expert_in = normalize(after_float, gain_ffn).astype(jnp.bfloat16)
-    gate_w = w_expert_gate[0]
-    up_w = w_expert_up[0]
-    down_w = w_expert_down[0]
     own_routes = lax.dynamic_slice_in_dim(routing, device_index * seq_rows, seq_rows, 0)
     route_weight = route_weights(expert_in, w_router, own_routes)
     flat_routes = own_routes.reshape(-1)
@@ -351,7 +425,9 @@
         "rp,rd->pd", dispatch, expert_in, preferred_element_type=jnp.float32
     ).astype(jnp.bfloat16)
     arrived = dispatch_rows(outgoing.reshape(experts, capacity, model_width), group_size)
-    computed = expert_quarter(arrived.reshape(-1, model_width), gate_w, up_w, down_w)
+    computed = expert_quarter(
+        arrived.reshape(-1, model_width), w_expert_gate, w_expert_up, w_expert_down
+    )
     returned = return_rows(computed.reshape(arrived.shape))
     summed = returned.astype(jnp.float32).reshape(experts * capacity, model_width)
     combine = jnp.sum(jnp.where(placed, route_weight[:, :, None], 0.0), axis=1)

time: 108 us -> 93.3 us (0.86)
  matrix products: 32.4 us -> 8.78 us
  local copies, waits for them, and re-layouts: 3.5 us -> 17 us
  other arithmetic: 15.1 us -> 6.46 us
  Pallas kernels: 55.9 us -> 59.5 us
    dot_general x3 -> x0, matrix products: 19.5 us -> none  [the longest x1 8.97 us: cell_step(): jnp.einsum('bhd,bhde->bhe', query_rows, cells_next, precision=lax.Precisi...]
    pallas_call x0 -> x2, Pallas kernels: none -> 11.4 us  [the longest x1 7.81 us: update_cells(): pl.pallas_call(cell_kernel, grid=(rows // block,), out_shape=(jax.ShapeDt...]
    unnamed x19 -> x47, local copies, waits for them, and re-layouts: 0.15 us -> 10.4 us
    add x1 -> x0, other arithmetic: 9.94 us -> none  [cell_step(): keep_weight[:, :, None, None] * memory_cells]
    pallas_call x1, Pallas kernels: 29.2 us -> 25.3 us  [dispatch_rows(): pl.pallas_call(functools.partial(dispatch_kernel, experts, group_size), o...]
    pallas_call x1, Pallas kernels: 26.7 us -> 22.8 us  [return_rows(): pl.pallas_call(functools.partial(return_kernel, experts, group_size), out...]
    unnamed x1 -> x0, other arithmetic: 2.2 us -> none
    dot_general x0 -> x1, other arithmetic: none -> 1.61 us  [cell_step(): jnp.einsum('bhd,bhd->bh', query_rows, norm_next, precision=lax.Precision....]
where the time goes in v2:
time: 93.3 us; the launch traced here: 92.8 us
  Pallas kernels  59.5 us (64%)
  local copies, waits for them, and re-layouts  17 us (18%)
  matrix products  8.78 us (9%)
  other arithmetic  6.46 us (7%)
  between operations  1.04 us (1%)
    pallas_call x1, Pallas kernels, dispatch_rows(): pl.pallas_call(functools.partial(dispatch_kernel, experts, group_size), o...  25.3 us
    pallas_call x1, Pallas kernels, return_rows(): pl.pallas_call(functools.partial(return_kernel, experts, group_size), out...  22.8 us
    unnamed x47, local copies, waits for them, and re-layouts  10.4 us
    pallas_call x1, Pallas kernels, update_cells(): pl.pallas_call(cell_kernel, grid=(rows // block,), out_shape=(jax.ShapeDt...  7.81 us
    pallas_call x1, Pallas kernels, expert_quarter(): pl.pallas_call(expert_kernel, out_shape=jax.ShapeDtypeStruct(rows_in.shap...  3.59 us
    dot_general x1, matrix products, cell_step(): jnp.dot(normed, w_value, preferred_element_type=jnp.float32)  3.2 us
    dot_general x1, matrix products, cell_step(): jnp.dot(normed, w_query, preferred_element_type=jnp.float32)  1.9 us
    mul x3, local copies, waits for them, and re-layouts, cell_step(): scaled_keys = write_weight[:, :, None] * key_rows  1.87 us

profile of v2, /device:TPU:0, one launch (start us, length us, event | category | flops | bytes accessed | tf_op | source)
XLA Modules:
  0.0 92.8 jit_solution(15024549077324620432)
XLA Ops:
  0.6 0.0 copy-start
  0.6 0.0 copy-start.7
  0.7 0.0 copy-start.9
  0.7 0.9 constant_dynamic-slice_fusion
  1.6 1.1 %fusion.1 = f32[32]{0:T(128)S(1)} fusion(bf16[32,2048]{1,0:T(8,128)(2,1)} %param.21), kind=kLoop, calls=%fused_computation.13 | loop fusion | flops 196576 | bytes 131200 | tf_op jit(solution)/shard_map/reduce_sum | solution.py:14
  2.7 0.1 copy.68
  2.8 0.1 eq.20
  2.9 0.8 copy.52
  3.7 1.3 %fusion.15 = f32[32,4]{1,0:T(8,128)S(1)} fusion(f32[32,4]{1,0:T(8,128)S(1)} %copy.52, bf16[2048,4]{0,1:T(4,128)(2,1)} %param.27, f32[4]{0:T(128)} %param.29, bf16[32,2048]{1,0:T(8,128)(2,1)} %param.21, f32[2048]{0:T(1024)} %param.22, f32[32]{0:T(128)S(1)} %add_rsqrt_fusion.3), kind=kOutput, calls=%fused_computation.37 | convolution fusion | flops 787712 | bytes 156816 | tf_op jit(solution)/shard_map/dot_general | solution.py:92
  5.0 1.9 %convolution_convert_fusion.3 = bf16[32,384]{1,0:T(8,128)(2,1)S(1)} fusion(bf16[2048,384]{1,0:T(8,128)(2,1)} %param.23, bf16[32,2048]{1,0:T(8,128)(2,1)} %param.21, f32[2048]{0:T(1024)} %param.22, f32[32]{0:T(128)S(1)} %add_rsqrt_fusion.3), kind=kOutput, calls=%fused_computation.3 | convolution fusion | flops 50606080 | bytes 1736832 | tf_op jit(solution)/shard_map/dot_general | solution.py:82
  7.0 0.4 convolution_convert_fusion.2
  7.4 0.1 fusion.13
  7.4 0.1 reduce_window_sum.11
  7.5 0.2 select_reduce_fusion.1
  7.7 0.1 reduce_sum.68
  7.8 0.1 copy.59
  7.9 0.7 fusion.12
  8.6 0.2 subtract_exponential_fusion
  8.9 0.7 copy.61
  9.5 3.2 %convolution_convert_fusion.1 = bf16[32,768]{1,0:T(8,128)(2,1)} fusion(bf16[2048,768]{1,0:T(8,128)(2,1)} %param.25, bf16[32,2048]{1,0:T(8,128)(2,1)S(1)} %copy-done.7, f32[2048]{0:T(1024)S(1)} %copy-done.9, f32[32]{0:T(128)S(1)} %add_rsqrt_fusion.3), kind=kOutput, calls=%fused_computation.1 | convolution fusion | flops 100950016 | bytes 3334272 | tf_op jit(solution)/shard_map/dot_general | solution.py:87
  12.7 0.6 reshape.94
  13.4 0.1 reshape.97
  13.5 0.1 mul.135
  13.6 1.6 %multiply_reduce_fusion.2 = (f32[32,4]{1,0:T(8,128)S(1)}, f32[32,4,96]{2,1,0:T(4,128)}) fusion(f32[32,4,96]{2,1,0:T(4,128)S(1)} %mul.135, f32[32,4,96]{2,1,0:T(4,128)S(1)} %reshape.97, f32[32,4]{1,0:T(8,128)S(1)} %get-tuple-element.28, f32[32,4,96]{2,1,0:T(4,128)} %param.31, f32[32,4]{1,0:T(8,128)S(1)} %subtract_exponential_fusion.1.keep), kind=kLoop, calls=%fused_computation.24 | loop fusion | flops 61312 | bytes 198144 | tf_op jit(solution)/shard_map/bhd,bhd->bh/dot_general | solution.py:103
  15.2 0.6 exponential_maximum_fusion
  15.8 0.1 mul.132
  15.9 0.1 mul.133
  16.0 0.8 copy_multiply_fusion
  16.8 0.9 %reshape.103.values = f32[32,4,192]{2,1,0:T(4,128)S(1)} reshape(bf16[32,768]{1,0:T(8,128)(2,1)} %convolution_convert_fusion.1) | data formatting | bytes 147456 | tf_op jit(solution)/shard_map/reshape | solution.py:87
  17.8 1.7 %copy.57 = f32[8,4,384]{1,2,0:T(8,128)} copy(f32[8,4,384]{2,0,1:T(8,128)S(1)} %copy_multiply_fusion) | data formatting | bytes 98304 | tf_op jit(solution)/shard_map/mul | solution.py:98
  19.5 1.6 %copy.54 = f32[8,4,384]{1,2,0:T(8,128)} copy(f32[8,4,384]{2,1,0:T(4,128)S(1)} %mul.131) | data formatting | bytes 98304 | tf_op jit(solution)/shard_map/mul | solution.py:83
  21.1 4.6 %copy-done.1 = f32[32,4,96,192]{3,2,1,0:T(8,128)S(1)} copy-done((f32[32,4,96,192]{3,2,1,0:T(8,128)S(1)}, f32[32,4,96,192]{3,2,1,0:T(8,128)}, u32[]{:S(2)}) %copy-start.1) | copy-done | bytes 9437208
  25.7 1.4 %copy-done.2 = f32[8,4,384]{1,2,0:T(8,128)S(1)} copy-done((f32[8,4,384]{1,2,0:T(8,128)S(1)}, f32[8,4,384]{1,2,0:T(8,128)}, u32[]{:S(2)}) %copy-start.2) | copy-done | bytes 49176
  27.1 1.4 %copy-done.3 = f32[8,4,384]{1,2,0:T(8,128)S(1)} copy-done((f32[8,4,384]{1,2,0:T(8,128)S(1)}, f32[8,4,384]{1,2,0:T(8,128)}, u32[]{:S(2)}) %copy-start.3) | copy-done | bytes 49176
  28.5 7.8 %update_cells.1 = (f32[32,4,96,192]{3,2,1,0:T(8,128)}, f32[32,4,192]{2,1,0:T(4,128)S(1)}) custom-call(f32[32,4]{1,0:T(8,128)S(1)} %subtract_exponential_fusion.1.keep, f32[32,4,96,192]{3,2,1,0:T(8,128)S(1)} %copy-done.1, f32[8,384,4]{2,1,0:T(8,128)S(1)} %bitcast.20, f32[8,384,4]{2,1,0:T(8,128)S(1)} %bitcast.19, f32[32,4,192]{2,1,0:T(4,128)S(1)} %reshape.103.values), custom_call_target="tpu_custom_call" | custom-call | tf_op jit(solution)/shard_map/update_cells/pallas_call | solution.py:48
  36.3 0.1 divide_convert_fusion
  36.4 0.1 convert_element_type.56
  36.6 0.7 multiply_reduce_fusion.1
  37.4 0.2 fusion.5
  37.6 0.2 fusion.10
  37.9 0.1 select_reduce_fusion
  38.1 0.4 convolution_convert_fusion
  38.4 25.3 %dispatch_rows.1 = bf16[8,4,16,2048]{3,2,1,0:T(8,128)(2,1)S(1)} custom-call(bf16[8,16,2048]{2,1,0:T(8,128)(2,1)S(1)} %bitcast.22), custom_call_target="tpu_custom_call" | custom-call | tf_op jit(solution)/shard_map/dispatch_rows/pallas_call | solution.py:245
  63.7 1.4 %copy-done.6 = bf16[1,384,2048]{2,1,0:T(8,128)(2,1)S(1)} copy-done((bf16[1,384,2048]{2,1,0:T(8,128)(2,1)S(1)}, bf16[1,384,2048]{2,1,0:T(8,128)(2,1)}, u32[]{:S(2)}) %copy-start.6) | copy-done | bytes 1572888
  65.1 3.6 %expert_quarter.1 = bf16[512,2048]{1,0:T(8,128)(2,1)S(1)} custom-call(bf16[512,2048]{1,0:T(8,128)(2,1)S(1)} %bitcast.17, bf16[1,2048,384]{2,1,0:T(8,128)(2,1)S(1)} %copy-done.4, bf16[1,2048,384]{2,1,0:T(8,128)(2,1)S(1)} %copy-done.5, bf16[1,384,2048]{2,1,0:T(8,128)(2,1)S(1)} %copy-done.6), custom_call_target="tpu_custom_call" | custom-call | tf_op jit(solution)/shard_map/expert_quarter/pallas_call | solution.py:233
  68.7 22.8 %return_rows.1 = bf16[8,16,2048]{2,1,0:T(8,128)(2,1)S(1)} custom-call(bf16[8,4,16,2048]{3,2,1,0:T(8,128)(2,1)S(1)} %bitcast.18), custom_call_target="tpu_custom_call" | custom-call | tf_op jit(solution)/shard_map/return_rows/pallas_call | solution.py:344
  91.6 0.4 multiply_reduce_fusion
  92.0 0.8 fusion.8
  (48 shorter events, 0.2 us)
Async XLA Ops:
  0.6 35.9 %copy-start = (bf16[768,2048]{1,0:T(8,128)(2,1)S(1)}, bf16[768,2048]{1,0:T(8,128)(2,1)}, u32[]{:S(2)}) copy-start(bf16[768,2048]{1,0:T(8,128)(2,1)} %param.33) | copy-start | bytes 9437188
  0.6 6.3 %copy-start.7 = (bf16[32,2048]{1,0:T(8,128)(2,1)S(1)}, bf16[32,2048]{1,0:T(8,128)(2,1)}, u32[]{:S(2)}) copy-start(bf16[32,2048]{1,0:T(8,128)(2,1)} %param.21) | copy-start | bytes 393220
  0.7 6.3 %copy-start.9 = (f32[2048]{0:T(1024)S(1)}, f32[2048]{0:T(1024)}, u32[]{:S(2)}) copy-start(f32[2048]{0:T(1024)} %param.22) | copy-start | bytes 24580
  1.6 1.2 %copy-start.14 = (s32[32,2]{0,1:T(2,128)}, s32[32,2]{0,1:T(2,128)S(1)}, u32[]{:S(2)}) copy-start(s32[32,2]{0,1:T(2,128)S(1)} %constant_dynamic-slice_fusion) | copy-start | bytes 772
  3.7 3.3 %copy-start.8 = (bf16[2048,384]{1,0:T(8,128)(2,1)S(1)}, bf16[2048,384]{1,0:T(8,128)(2,1)}, u32[]{:S(2)}) copy-start(bf16[2048,384]{1,0:T(8,128)(2,1)} %param.24) | copy-start | bytes 4718596
  5.0 3.6 %copy-start.20 = (bf16[2048,4]{0,1:T(4,128)(2,1)S(1)}, bf16[2048,4]{0,1:T(4,128)(2,1)}, u32[]{:S(2)}) copy-start(bf16[2048,4]{0,1:T(4,128)(2,1)} %param.26) | copy-start | bytes 49156
  5.0 3.6 %copy-start.21 = (f32[4]{0:T(128)S(1)}, f32[4]{0:T(128)}, u32[]{:S(2)}) copy-start(f32[4]{0:T(128)} %param.28) | copy-start | bytes 52
  7.9 0.9 %copy-start.12 = (s32[32,2]{0,1:T(2,128)}, s32[32,2]{0,1:T(2,128)S(1)}, u32[]{:S(2)}) copy-start(s32[32,2]{0,1:T(2,128)S(1)} %copy.59) | copy-start | bytes 772
  21.1 4.6 %copy-start.1 = (f32[32,4,96,192]{3,2,1,0:T(8,128)S(1)}, f32[32,4,96,192]{3,2,1,0:T(8,128)}, u32[]{:S(2)}) copy-start(f32[32,4,96,192]{3,2,1,0:T(8,128)} %cells.1) | copy-start | bytes 28311556
  25.7 1.4 %copy-start.2 = (f32[8,4,384]{1,2,0:T(8,128)S(1)}, f32[8,4,384]{1,2,0:T(8,128)}, u32[]{:S(2)}) copy-start(f32[8,4,384]{1,2,0:T(8,128)} %copy.57) | copy-start | bytes 147460
  27.1 1.4 %copy-start.3 = (f32[8,4,384]{1,2,0:T(8,128)S(1)}, f32[8,4,384]{1,2,0:T(8,128)}, u32[]{:S(2)}) copy-start(f32[8,4,384]{1,2,0:T(8,128)} %copy.54) | copy-start | bytes 147460
  28.5 7.8 %copy-start.10 = (f32[32,4]{1,0:T(8,128)S(1)}, f32[32,4]{1,0:T(8,128)}, u32[]{:S(2)}) copy-start(f32[32,4]{1,0:T(8,128)} %exponential_maximum_fusion) | copy-start | bytes 1540
  36.5 0.8 copy-start.16
  36.6 1.1 %copy-start.17 = (f32[2048]{0:T(1024)S(1)}, f32[2048]{0:T(1024)}, u32[]{:S(2)}) copy-start(f32[2048]{0:T(1024)} %param.35) | copy-start | bytes 24580
  36.6 1.1 %copy-start.19 = (bf16[2048,8]{0,1:T(8,128)(2,1)S(1)}, bf16[2048,8]{0,1:T(8,128)(2,1)}, u32[]{:S(2)}) copy-start(bf16[2048,8]{0,1:T(8,128)(2,1)} %param.36) | copy-start | bytes 98308
  36.6 1.3 %copy-start.15 = (s32[32,2]{0,1:T(2,128)S(1)}, s32[32,2]{0,1:T(2,128)}, u32[]{:S(2)}) copy-start(s32[32,2]{0,1:T(2,128)} %copy-done.14) | copy-start | bytes 772
  36.6 1.3 %copy-start.13 = (s32[32,2]{0,1:T(2,128)S(1)}, s32[32,2]{0,1:T(2,128)}, u32[]{:S(2)}) copy-start(s32[32,2]{0,1:T(2,128)} %copy-done.12) | copy-start | bytes 772
  36.6 1.4 %copy-start.11 = (pred[32,128]{1,0:T(8,128)(4,1)S(1)}, pred[32,128]{1,0:T(8,128)(4,1)}, u32[]{:S(2)}) copy-start(pred[32,128]{1,0:T(8,128)(4,1)} %fusion.12) | copy-start | bytes 12292
  38.0 25.7 %copy-start.4 = (bf16[1,2048,384]{2,1,0:T(8,128)(2,1)S(1)}, bf16[1,2048,384]{2,1,0:T(8,128)(2,1)}, u32[]{:S(2)}) copy-start(bf16[1,2048,384]{2,1,0:T(8,128)(2,1)} %gate_w.1) | copy-start | bytes 4718596
  38.1 25.7 %copy-start.5 = (bf16[1,2048,384]{2,1,0:T(8,128)(2,1)S(1)}, bf16[1,2048,384]{2,1,0:T(8,128)(2,1)}, u32[]{:S(2)}) copy-start(bf16[1,2048,384]{2,1,0:T(8,128)(2,1)} %up_w.1) | copy-start | bytes 4718596
  63.7 1.4 %copy-start.6 = (bf16[1,384,2048]{2,1,0:T(8,128)(2,1)S(1)}, bf16[1,384,2048]{2,1,0:T(8,128)(2,1)}, u32[]{:S(2)}) copy-start(bf16[1,384,2048]{2,1,0:T(8,128)(2,1)} %down_w.1) | copy-start | bytes 4718596
  68.7 23.3 %copy-start.18 = (f32[2048]{0:T(1024)S(1)}, f32[2048]{0:T(1024)}, u32[]{:S(2)}) copy-start(f32[2048]{0:T(1024)} %param.41) | copy-start | bytes 24580

commit v3 on v2

--- a/solution.py
+++ b/solution.py
@@ -60,7 +60,7 @@
             value_spec,
         ],
         out_specs=(cell_spec, value_spec),
-        compiler_params=pltpu.CompilerParams(vmem_limit_bytes=16 * 2**20),
+        compiler_params=pltpu.CompilerParams(vmem_limit_bytes=56 * 2**20),
         name="update_cells",
     )(keep, cells, columns(queries), columns(keys), values)
 

time: 93.3 us -> 94 us (level)
  local copies, waits for them, and re-layouts: 17 us -> 10.9 us
  Pallas kernels: 59.5 us -> 64.8 us
    unnamed x47 -> x41, local copies, waits for them, and re-layouts: 10.4 us -> 3.55 us
    pallas_call x1, Pallas kernels: 7.81 us -> 13.2 us  [update_cells(): pl.pallas_call(cell_kernel, grid=(rows // block,), out_shape=(jax.ShapeDt...]
where the time goes in v3:
time: 94 us; the launch traced here: 93.5 us
  Pallas kernels  64.8 us (69%)
  local copies, waits for them, and re-layouts  10.9 us (12%)
  matrix products  9.4 us (10%)
  other arithmetic  7.25 us (8%)
  between operations  1.02 us (1%)
    pallas_call x1, Pallas kernels, dispatch_rows(): pl.pallas_call(functools.partial(dispatch_kernel, experts, group_size), o...  25.3 us
    pallas_call x1, Pallas kernels, return_rows(): pl.pallas_call(functools.partial(return_kernel, experts, group_size), out...  22.8 us
    pallas_call x1, Pallas kernels, update_cells(): pl.pallas_call(cell_kernel, grid=(rows // block,), out_shape=(jax.ShapeDt...  13.2 us
    pallas_call x1, Pallas kernels, expert_quarter(): pl.pallas_call(expert_kernel, out_shape=jax.ShapeDtypeStruct(rows_in.shap...  3.59 us
    unnamed x41, local copies, waits for them, and re-layouts  3.55 us
    dot_general x1, matrix products, cell_step(): jnp.dot(normed, w_value, preferred_element_type=jnp.float32)  3.2 us
    mul x3, local copies, waits for them, and re-layouts, cell_step(): scaled_keys = write_weight[:, :, None] * key_rows  2.58 us
    dot_general x1, matrix products, cell_step(): jnp.dot(normed, w_query, preferred_element_type=jnp.float32)  1.9 us

profile of v3, /device:TPU:0, one launch (start us, length us, event | category | flops | bytes accessed | tf_op | source)
XLA Modules:
  0.0 93.5 jit_solution(7081907653642450087)
XLA Ops:
  0.6 0.0 copy-start
  0.6 0.0 copy-start.4
  0.7 0.9 constant_dynamic-slice_fusion
  1.6 1.1 %fusion.1 = f32[32]{0:T(128)S(1)} fusion(bf16[32,2048]{1,0:T(8,128)(2,1)} %param.21), kind=kLoop, calls=%fused_computation.13 | loop fusion | flops 196576 | bytes 131200 | tf_op jit(solution)/shard_map/reduce_sum | solution.py:14
  2.7 0.1 copy.68
  2.8 0.1 eq.20
  2.9 0.8 copy.52
  3.7 1.3 %fusion.15 = f32[32,4]{1,0:T(8,128)S(1)} fusion(f32[32,4]{1,0:T(8,128)S(1)} %copy.52, bf16[2048,4]{0,1:T(4,128)(2,1)} %param.27, f32[4]{0:T(128)} %param.29, bf16[32,2048]{1,0:T(8,128)(2,1)} %param.21, f32[2048]{0:T(1024)} %param.22, f32[32]{0:T(128)S(1)} %add_rsqrt_fusion.3), kind=kOutput, calls=%fused_computation.37 | convolution fusion | flops 787712 | bytes 156816 | tf_op jit(solution)/shard_map/dot_general | solution.py:92
  5.0 1.9 %convolution_convert_fusion.3 = bf16[32,384]{1,0:T(8,128)(2,1)S(1)} fusion(bf16[2048,384]{1,0:T(8,128)(2,1)} %param.23, bf16[32,2048]{1,0:T(8,128)(2,1)} %param.21, f32[2048]{0:T(1024)} %param.22, f32[32]{0:T(128)S(1)} %add_rsqrt_fusion.3), kind=kOutput, calls=%fused_computation.3 | convolution fusion | flops 50606080 | bytes 1736832 | tf_op jit(solution)/shard_map/dot_general | solution.py:82
  7.0 0.4 convolution_convert_fusion.2
  7.4 0.1 fusion.13
  7.4 0.1 reduce_window_sum.11
  7.5 0.2 select_reduce_fusion.1
  7.7 0.1 reduce_sum.68
  7.8 0.1 copy.59
  7.9 0.5 copy-done.9
  8.5 0.7 fusion.12
  9.1 0.8 subtract_exponential_fusion
  10.0 0.6 subtract_exponential_fusion.1.keep
  10.6 0.7 copy.61
  11.2 3.2 %convolution_convert_fusion.1 = bf16[32,768]{1,0:T(8,128)(2,1)} fusion(bf16[2048,768]{1,0:T(8,128)(2,1)} %param.25, bf16[32,2048]{1,0:T(8,128)(2,1)S(1)} %copy-done.4, f32[2048]{0:T(1024)S(1)} %copy-done.7, f32[32]{0:T(128)S(1)} %add_rsqrt_fusion.3), kind=kOutput, calls=%fused_computation.1 | convolution fusion | flops 100950016 | bytes 3334272 | tf_op jit(solution)/shard_map/dot_general | solution.py:87
  14.5 0.1 reshape.97
  14.6 0.1 mul.135
  14.7 1.6 %multiply_reduce_fusion.2 = (f32[32,4]{1,0:T(8,128)S(1)}, f32[32,4,96]{2,1,0:T(4,128)}) fusion(f32[32,4,96]{2,1,0:T(4,128)S(1)} %mul.135, f32[32,4,96]{2,1,0:T(4,128)S(1)} %reshape.97, f32[32,4]{1,0:T(8,128)} %get-tuple-element.28, f32[32,4,96]{2,1,0:T(4,128)} %param.31, f32[32,4]{1,0:T(8,128)} %subtract_exponential_fusion.1.keep), kind=kLoop, calls=%fused_computation.24 | loop fusion | flops 61312 | bytes 198144 | tf_op jit(solution)/shard_map/bhd,bhd->bh/dot_general | solution.py:103
  16.3 0.7 exponential_maximum_fusion
  17.0 0.8 mul.132
  17.8 0.1 mul.133
  18.0 1.6 %reshape.103.values = f32[32,4,192]{2,1,0:T(4,128)} reshape(bf16[32,768]{1,0:T(8,128)(2,1)} %convolution_convert_fusion.1) | data formatting | bytes 147456 | tf_op jit(solution)/shard_map/reshape | solution.py:87
  19.6 1.7 %copy.57 = f32[8,4,384]{1,2,0:T(8,128)} copy(f32[8,4,384]{2,0,1:T(8,128)S(1)} %copy_multiply_fusion) | data formatting | bytes 98304 | tf_op jit(solution)/shard_map/mul | solution.py:98
  21.2 1.7 %copy.54 = f32[8,4,384]{1,2,0:T(8,128)} copy(f32[8,4,384]{2,1,0:T(4,128)S(1)} %mul.131) | data formatting | bytes 98304 | tf_op jit(solution)/shard_map/mul | solution.py:83
  22.9 13.2 %update_cells.1 = (f32[32,4,96,192]{3,2,1,0:T(8,128)}, f32[32,4,192]{2,1,0:T(4,128)}) custom-call(f32[32,4]{1,0:T(8,128)} %subtract_exponential_fusion.1.keep, f32[32,4,96,192]{3,2,1,0:T(8,128)} %cells.1, f32[8,384,4]{2,1,0:T(8,128)} %bitcast.22, f32[8,384,4]{2,1,0:T(8,128)} %bitcast.21, f32[32,4,192]{2,1,0:T(4,128)} %reshape.103.values), custom_call_target="tpu_custom_call" | custom-call | tf_op jit(solution)/shard_map/update_cells/pallas_call | solution.py:48
  36.1 1.0 %divide_convert_fusion = bf16[32,4,192]{2,1,0:T(4,128)(2,1)S(1)} fusion(f32[32,4,192]{2,1,0:T(4,128)} %get-tuple-element.6, f32[32,4]{1,0:T(8,128)S(1)} %exponential_maximum_fusion), kind=kLoop, calls=%fused_computation.23 | loop fusion | flops 49152 | bytes 147968 | tf_op jit(solution)/shard_map/convert_element_type | solution.py:108
  37.1 0.1 convert_element_type.56
  37.2 0.0 copy-start.16
  37.3 0.7 multiply_reduce_fusion.1
  38.1 0.2 fusion.5
  38.3 0.2 fusion.10
  38.6 0.1 select_reduce_fusion
  38.7 0.0 copy-start.1
  38.7 0.4 convolution_convert_fusion
  39.1 25.3 %dispatch_rows.1 = bf16[8,4,16,2048]{3,2,1,0:T(8,128)(2,1)S(1)} custom-call(bf16[8,16,2048]{2,1,0:T(8,128)(2,1)S(1)} %bitcast.20), custom_call_target="tpu_custom_call" | custom-call | tf_op jit(solution)/shard_map/dispatch_rows/pallas_call | solution.py:245
  64.4 0.0 copy-start.3
  64.4 1.4 %copy-done.3 = bf16[1,384,2048]{2,1,0:T(8,128)(2,1)S(1)} copy-done((bf16[1,384,2048]{2,1,0:T(8,128)(2,1)S(1)}, bf16[1,384,2048]{2,1,0:T(8,128)(2,1)}, u32[]{:S(2)}) %copy-start.3) | copy-done | bytes 1572888
  65.8 3.6 %expert_quarter.1 = bf16[512,2048]{1,0:T(8,128)(2,1)S(1)} custom-call(bf16[512,2048]{1,0:T(8,128)(2,1)S(1)} %bitcast.17, bf16[1,2048,384]{2,1,0:T(8,128)(2,1)S(1)} %copy-done.1, bf16[1,2048,384]{2,1,0:T(8,128)(2,1)S(1)} %copy-done.2, bf16[1,384,2048]{2,1,0:T(8,128)(2,1)S(1)} %copy-done.3), custom_call_target="tpu_custom_call" | custom-call | tf_op jit(solution)/shard_map/expert_quarter/pallas_call | solution.py:233
  69.4 0.0 copy-start.15
  69.4 22.8 %return_rows.1 = bf16[8,16,2048]{2,1,0:T(8,128)(2,1)S(1)} custom-call(bf16[8,4,16,2048]{3,2,1,0:T(8,128)(2,1)S(1)} %bitcast.18), custom_call_target="tpu_custom_call" | custom-call | tf_op jit(solution)/shard_map/return_rows/pallas_call | solution.py:344
  92.2 0.4 multiply_reduce_fusion
  92.7 0.8 fusion.8
  (42 shorter events, 0.2 us)
Async XLA Ops:
  0.6 36.6 %copy-start = (bf16[768,2048]{1,0:T(8,128)(2,1)S(1)}, bf16[768,2048]{1,0:T(8,128)(2,1)}, u32[]{:S(2)}) copy-start(bf16[768,2048]{1,0:T(8,128)(2,1)} %param.33) | copy-start | bytes 9437188
  0.6 6.3 %copy-start.4 = (bf16[32,2048]{1,0:T(8,128)(2,1)S(1)}, bf16[32,2048]{1,0:T(8,128)(2,1)}, u32[]{:S(2)}) copy-start(bf16[32,2048]{1,0:T(8,128)(2,1)} %param.21) | copy-start | bytes 393220
  0.7 6.3 %copy-start.7 = (f32[2048]{0:T(1024)S(1)}, f32[2048]{0:T(1024)}, u32[]{:S(2)}) copy-start(f32[2048]{0:T(1024)} %param.22) | copy-start | bytes 24580
  1.6 1.2 %copy-start.11 = (s32[32,2]{0,1:T(2,128)}, s32[32,2]{0,1:T(2,128)S(1)}, u32[]{:S(2)}) copy-start(s32[32,2]{0,1:T(2,128)S(1)} %constant_dynamic-slice_fusion) | copy-start | bytes 772
  3.7 3.3 %copy-start.5 = (bf16[2048,384]{1,0:T(8,128)(2,1)S(1)}, bf16[2048,384]{1,0:T(8,128)(2,1)}, u32[]{:S(2)}) copy-start(bf16[2048,384]{1,0:T(8,128)(2,1)} %param.24) | copy-start | bytes 4718596
  5.0 4.1 %copy-start.17 = (bf16[2048,4]{0,1:T(4,128)(2,1)S(1)}, bf16[2048,4]{0,1:T(4,128)(2,1)}, u32[]{:S(2)}) copy-start(bf16[2048,4]{0,1:T(4,128)(2,1)} %param.26) | copy-start | bytes 49156
  5.0 4.1 %copy-start.18 = (f32[4]{0:T(128)S(1)}, f32[4]{0:T(128)}, u32[]{:S(2)}) copy-start(f32[4]{0:T(128)} %param.28) | copy-start | bytes 52
  7.9 0.5 copy-start.9
  10.0 4.5 %copy-start.6 = (f32[32,4]{1,0:T(8,128)}, f32[32,4]{1,0:T(8,128)S(1)}, u32[]{:S(2)}) copy-start(f32[32,4]{1,0:T(8,128)S(1)} %get-tuple-element.29) | copy-start | bytes 1540
  37.2 0.8 copy-start.13
  37.2 1.1 %copy-start.14 = (f32[2048]{0:T(1024)S(1)}, f32[2048]{0:T(1024)}, u32[]{:S(2)}) copy-start(f32[2048]{0:T(1024)} %param.35) | copy-start | bytes 24580
  37.2 1.1 %copy-start.16 = (bf16[2048,8]{0,1:T(8,128)(2,1)S(1)}, bf16[2048,8]{0,1:T(8,128)(2,1)}, u32[]{:S(2)}) copy-start(bf16[2048,8]{0,1:T(8,128)(2,1)} %param.36) | copy-start | bytes 98308
  37.2 1.3 %copy-start.12 = (s32[32,2]{0,1:T(2,128)S(1)}, s32[32,2]{0,1:T(2,128)}, u32[]{:S(2)}) copy-start(s32[32,2]{0,1:T(2,128)} %copy-done.11) | copy-start | bytes 772
  37.3 1.3 %copy-start.10 = (s32[32,2]{0,1:T(2,128)S(1)}, s32[32,2]{0,1:T(2,128)}, u32[]{:S(2)}) copy-start(s32[32,2]{0,1:T(2,128)} %copy-done.9) | copy-start | bytes 772
  37.3 1.4 %copy-start.8 = (pred[32,128]{1,0:T(8,128)(4,1)S(1)}, pred[32,128]{1,0:T(8,128)(4,1)}, u32[]{:S(2)}) copy-start(pred[32,128]{1,0:T(8,128)(4,1)} %fusion.12) | copy-start | bytes 12292
  38.7 25.7 %copy-start.1 = (bf16[1,2048,384]{2,1,0:T(8,128)(2,1)S(1)}, bf16[1,2048,384]{2,1,0:T(8,128)(2,1)}, u32[]{:S(2)}) copy-start(bf16[1,2048,384]{2,1,0:T(8,128)(2,1)} %gate_w.1) | copy-start | bytes 4718596
  38.7 25.7 %copy-start.2 = (bf16[1,2048,384]{2,1,0:T(8,128)(2,1)S(1)}, bf16[1,2048,384]{2,1,0:T(8,128)(2,1)}, u32[]{:S(2)}) copy-start(bf16[1,2048,384]{2,1,0:T(8,128)(2,1)} %up_w.1) | copy-start | bytes 4718596
  64.4 1.4 %copy-start.3 = (bf16[1,384,2048]{2,1,0:T(8,128)(2,1)S(1)}, bf16[1,384,2048]{2,1,0:T(8,128)(2,1)}, u32[]{:S(2)}) copy-start(bf16[1,384,2048]{2,1,0:T(8,128)(2,1)} %down_w.1) | copy-start | bytes 4718596
  69.4 23.3 %copy-start.15 = (f32[2048]{0:T(1024)S(1)}, f32[2048]{0:T(1024)}, u32[]{:S(2)}) copy-start(f32[2048]{0:T(1024)} %param.41) | copy-start | bytes 24580
